TPU v7x, 32 devices: a whole 2x2x4 slice. The times are simulated.
32 devices in a mesh: sp: 8 (over z, y), tp: 4 (over x, core).
Axes of the slice: x: 2, y: 2, z: 4, core: 2. Of those that a mesh axis runs over, the one named last changes fastest.
Arguments:
- tokens: bfloat16 [4096, 2048], P('sp', 'tp'), may hold values from -400 to 400
- norm_gain: float32 [2048], replicated, may hold values from 0.1 to 1.9
- query_weight: bfloat16 [2048, 1024], P(None, 'tp'), may hold values from -0.37306796 to 0.37306796
- key_weight: bfloat16 [2048, 1024], P(None, 'tp'), may hold values from -0.2625825 to 0.2625825
- value_weight: bfloat16 [2048, 1024], P(None, 'tp'), may hold values from -0.125 to 0.125
- outer_gate_weight: bfloat16 [2048, 1024], P(None, 'tp'), may hold values from -0.125 to 0.125
- inner_gate_weight: bfloat16 [2048, 1024], P(None, 'tp'), may hold values from -0.125 to 0.125
- conv_input_weight: bfloat16 [2048, 1024], P(None, 'tp'), may hold values from -0.125 to 0.125
- conv_taps: float32 [3, 1024], P(None, 'tp'), may hold values from -3.5 to 3.5
- lambdas: float32 [8], P('tp'), may hold values from 0.3 to 0.8
- head_gain: float32 [128], replicated, may hold values from 0.1 to 1.9
- attn_out_weight: bfloat16 [1024, 2048], P(None, 'tp'), may hold values from -0.125 to 0.125
- conv_out_weight: bfloat16 [1024, 2048], P(None, 'tp'), may hold values from -0.125 to 0.125
Outputs:
- mixed_out: bfloat16 [4096, 2048], P('sp', 'tp')
- log_totals: float32 [8, 2, 4096], P('tp', None, 'sp')
All inputs are finite; a program needn't handle non-finite values.
Results may differ from a plain program's by a relative error of at most 0.014.
The roundings to bfloat16 on the way count: a program that leaves them out, or rounds other values in their place, can miss the bound.
Values may be sent and summed in bfloat16 or wider, within the bound.
A program may use at most 128 MiB of HBM per device.

v0:
```python
import functools

import jax
import jax.numpy as jnp
import numpy as np
from jax import lax
from jax.experimental import pallas as pl
from jax.experimental.pallas import tpu as pltpu
from jax.sharding import PartitionSpec as P

NORM_EPS = 1e-06
HEAD_EPS = 1e-05
ROPE_BASE = 500000.0
MASKED = -1e30
HEAD_SCALE = 0.8
F32 = jnp.float32
BF16 = jnp.bfloat16


def dot(a, b):
    return jnp.dot(a, b, preferred_element_type=F32)


def dot_t(a, b):
    return lax.dot_general(a, b, (((1,), (1,)), ((), ())), preferred_element_type=F32)


def kernel(
    dims,
    tokens,
    gain,
    freq,
    wq_h,
    wk_h,
    wv_h,
    wo_h,
    wi_h,
    ws_h,
    taps,
    lambdas,
    head_gain,
    wa_h,
    wc_h,
    out,
    lse,
    tok,
    scaled,
    inv,
    cos_t,
    sin_t,
    wq,
    wk,
    wv,
    wo,
    wi,
    ws,
    wa,
    wc,
    kv,
    qz,
    row_max,
    row_sum,
    acc,
    gate,
    padded,
    tail,
    rim,
    conv_all,
    attn_all,
    total,
    w_sem,
    own_sem,
    tok_recv,
    tok_send,
    tok_relay,
    kv_recv,
    kv_send_z,
    kv_send_y,
    kv_extra,
    rim_sem,
    mix_recv,
    mix_send,
    mix_relay,
):
    S, T, Z, Y, H = dims["S"], dims["T"], dims["Z"], dims["Y"], dims["H"]
    L, Dt = tokens.shape
    Wd = T * Dt
    C = wq_h.shape[1]
    V = C // H
    hd = V // 2
    NR = tok_recv.shape[1]
    R = L // NR
    NM = mix_recv.shape[2]
    M = L // NM
    X = T // 2
    taps_n = taps.shape[0]
    PAD = tail.shape[0]

    sp = lax.axis_index("sp")
    tp = lax.axis_index("tp")
    z = sp // Y
    y = sp % Y
    core = tp % 2
    xi = tp // 2
    sib = xi * 2 + (1 - core)

    def peer(k):
        return ((xi + k) % X) * 2 + core

    def source(k):
        return ((xi - k + X) % X) * 2 + core

    pairs = [(wk_h, wk), (wv_h, wv), (wq_h, wq), (wi_h, wi), (ws_h, ws), (wo_h, wo), (wc_h, wc), (wa_h, wa)]
    own = pltpu.make_async_copy(tokens, tok.at[tp], own_sem)
    own.start()
    loads = [pltpu.make_async_copy(s, d, w_sem.at[i]) for i, (s, d) in enumerate(pairs)]
    for load in loads:
        load.start()

    barrier = pltpu.get_barrier_semaphore()

    def greet(target):
        pl.semaphore_signal(barrier, inc=1, device_id=target)

    for k in range(1, T):
        greet({"tp": (tp + k) % T})
    for k in range(1, Y):
        greet({"sp": z * Y + (y + k) % Y})
    has_up = z + 1 < Z
    has_down = z > 0
    far_up = jnp.logical_and(has_up, y == Y - 1) if Y > 1 else None
    far_down = jnp.logical_and(has_down, y == 0) if Y > 1 else None
    expect = (T - 1) + (Y - 1) + has_up.astype(jnp.int32) + has_down.astype(jnp.int32)

    @pl.when(has_up)
    def _():
        greet({"sp": sp + Y})

    @pl.when(has_down)
    def _():
        greet({"sp": sp - Y})

    if Y > 1:
        expect = expect + far_up.astype(jnp.int32) + far_down.astype(jnp.int32)

        @pl.when(far_up)
        def _():
            greet({"sp": sp + 1})

        @pl.when(far_down)
        def _():
            greet({"sp": sp - 1})

    pl.semaphore_wait(barrier, expect)

    def tok_rows(r):
        return pl.ds(pl.multiple_of(r * R, R), R)

    def tok_copy(src, piece, r, send, target):
        return pltpu.make_async_remote_copy(
            src_ref=src,
            dst_ref=tok.at[piece, tok_rows(r), :],
            send_sem=send,
            recv_sem=tok_recv.at[piece, r],
            device_id={"tp": target},
        )

    def tok_own(k, r):
        target = peer(k) if k else sib
        return tok_copy(tokens.at[tok_rows(r), :], tp, r, tok_send.at[k, r], target)

    def tok_forward(k, r):
        piece = source(k)
        return tok_copy(tok.at[piece, tok_rows(r), :], piece, r, tok_relay.at[k, r], sib)

    def tok_wait(piece, r):
        tok_copy(tok.at[piece, tok_rows(r), :], piece, r, tok_send.at[0, r], sib).wait_recv()

    for r in range(NR):
        for k in list(range(1, X)) + [0]:
            tok_own(k, r).start()

    lane = lax.broadcasted_iota(jnp.int32, (R, V), 1)
    first = (lane % hd) < (hd // 2)

    def table(r, carry):
        base = sp * L + r * R
        pos = (base + lax.broadcasted_iota(jnp.int32, (R, V), 0)).astype(F32)
        angle = pos * freq[...]
        sine = jnp.sin(angle)
        cos_t[tok_rows(r), :] = jnp.cos(angle)
        sin_t[tok_rows(r), :] = jnp.where(first, -sine, sine)
        return carry

    lax.fori_loop(0, NR, table, 0)

    def rotate(block, rows):
        low = (lax.broadcasted_iota(jnp.int32, block.shape, 1) % hd) < (hd // 2)
        other = jnp.where(
            low, pltpu.roll(block, V - hd // 2, 1), pltpu.roll(block, hd // 2, 1)
        )
        return block * cos_t[rows, :] + other * sin_t[rows, :]

    def kv_copy(j, r, send, target):
        block = kv.at[j, tok_rows(r), :]
        return pltpu.make_async_remote_copy(
            src_ref=block,
            dst_ref=block,
            send_sem=send,
            recv_sem=kv_recv.at[j, r],
            device_id={"sp": target},
        )

    def kv_up(dz, r):
        return kv_copy(sp - dz * Y, r, kv_send_z.at[dz, r], sp + Y)

    def kv_side(dz, r, k):
        return kv_copy(sp - dz * Y, r, kv_send_y.at[dz, r, k - 1], z * Y + (y + k) % Y)

    def kv_wait(j, r):
        kv_copy(j, r, kv_send_z.at[0, r], sp).wait_recv()

    EX = NR // 2 if Y == 2 else 0

    def extra(r):
        return kv_copy(0, r, kv_extra.at[r], sp + Y)

    def kv_send(dz, r, act):
        @pl.when(has_up)
        def _():
            act(kv_up(dz, r))

        for k in range(1, Y):
            wanted = jnp.logical_or(dz > 0, y + k < Y)
            if EX:
                other_way = jnp.logical_and(dz == z, jnp.logical_and(dz > 0, r < EX))
                wanted = jnp.logical_and(wanted, jnp.logical_not(jnp.logical_and(y == 0, other_way)))

            @pl.when(wanted)
            def _():
                act(kv_side(dz, r, k))

    def relay(dz, r):
        @pl.when(dz <= z)
        def _():
            kv_wait(sp - dz * Y, r)
            kv_send(dz, r, lambda copy: copy.start())

    def first_relay(r):
        relay(1, r)
        if EX:

            @pl.when(jnp.logical_and(jnp.logical_and(z == 0, y == 1), r < EX))
            def _():
                kv_wait(0, r)

                @pl.when(has_up)
                def _():
                    extra(r).start()

    own.wait()
    loads[0].wait()
    loads[1].wait()

    def key_chunk(r, carry):
        rows = tok_rows(r)
        for k in range(1, X):
            tok_wait(source(k), r)
            tok_forward(k, r).start()
        tok_wait(sib, r)
        for k in range(1, X):
            tok_wait(((xi + k) % X) * 2 + (1 - core), r)
        squares = jnp.zeros((R, 1), F32)
        for t in range(T):
            block = tok[t, rows, :].astype(F32)
            squares = squares + jnp.sum(block * block, axis=1, keepdims=True)
            scaled[rows, t * Dt : (t + 1) * Dt] = (block * gain[:, t * Dt : (t + 1) * Dt]).astype(BF16)
        inverse = lax.rsqrt(squares / Wd + NORM_EPS)
        inv[rows, :] = inverse
        left = scaled[rows, :]
        keys = inverse * dot(left, wk[...])
        for h in range(H):
            kv[sp, rows, h * V : (h + 1) * V] = rotate(keys[:, h * V : (h + 1) * V], rows).astype(BF16)
        kv[sp, rows, C : 2 * C] = (inverse * dot(left, wv[...])).astype(BF16)
        kv_send(0, r, lambda copy: copy.start())

        @pl.when(r > 0)
        def _():
            first_relay(r - 1)

        return carry

    lax.fori_loop(0, NR, key_chunk, 0)

    for load in loads[2:6]:
        load.wait()
    half = lax.broadcasted_iota(jnp.int32, (M, V), 1) < hd
    scale = hd ** (-0.5)

    def mix_rows(r):
        return pl.ds(pl.multiple_of(r * M, M), M)

    def query_chunk(r, carry):
        rows = mix_rows(r)
        inverse = inv[rows, :]
        left = scaled[rows, :]
        queries = inverse * dot(left, wq[...])
        for h in range(H):
            turned = rotate(queries[:, h * V : (h + 1) * V], rows).astype(BF16).astype(F32) * scale
            qz[h, 0, rows, :] = jnp.where(half, turned, 0.0).astype(BF16)
            qz[h, 1, rows, :] = jnp.where(half, 0.0, turned).astype(BF16)
        inner = (inverse * dot(left, wi[...])).astype(BF16)
        signal = (inverse * dot(left, ws[...])).astype(BF16)
        conv_in = (inner.astype(F32) * signal.astype(F32)).astype(BF16)
        padded[pl.ds(pl.multiple_of(PAD + r * M, PAD), M), :] = conv_in.astype(F32)
        gate[rows, :] = (inverse * dot(left, wo[...])).astype(BF16)

        @pl.when(r == 0)
        def _():
            first_relay(NR - 1)

        return carry

    lax.fori_loop(0, NM, query_chunk, 0)
    tail[...] = padded[L : L + PAD, :].astype(BF16)
    rim_copy = pltpu.make_async_remote_copy(
        src_ref=tail,
        dst_ref=rim,
        send_sem=rim_sem.at[0],
        recv_sem=rim_sem.at[1],
        device_id={"sp": (sp + 1) % S},
    )

    @pl.when(sp + 1 < S)
    def _():
        rim_copy.start()

    def attend(j, diagonal):
        def one(i, carry):
            rows = mix_rows(i)
            for h in range(H):
                query = qz[h, :, rows, :].reshape(2 * M, V)
                scores = dot_t(query, kv[j, :, h * V : (h + 1) * V])
                if diagonal:
                    row = lax.broadcasted_iota(jnp.int32, scores.shape, 0)
                    row = jnp.where(row >= M, row - M, row) + i * M
                    col = lax.broadcasted_iota(jnp.int32, scores.shape, 1)
                    scores = jnp.where(row >= col, scores, MASKED)
                    new_max = jnp.max(scores, axis=1, keepdims=True)
                else:
                    old_max = row_max[h, :, rows, :].reshape(2 * M, 1)
                    new_max = jnp.maximum(old_max, jnp.max(scores, axis=1, keepdims=True))
                weights = jnp.exp(scores - new_max)
                sums = jnp.sum(weights, axis=1, keepdims=True)
                mixed = dot(weights.astype(BF16), kv[j, :, C + h * V : C + (h + 1) * V])
                if not diagonal:
                    fade = jnp.exp(old_max - new_max)
                    sums = sums + fade * row_sum[h, :, rows, :].reshape(2 * M, 1)
                    mixed = mixed + fade * acc[h, :, rows, :].reshape(2 * M, V)
                row_max[h, :, rows, :] = new_max.reshape(2, M, 1)
                row_sum[h, :, rows, :] = sums.reshape(2, M, 1)
                acc[h, :, rows, :] = mixed.reshape(2, M, V)
            return carry

        lax.fori_loop(0, NM, one, 0)

    attend(sp, True)

    @pl.when(sp > 0)
    def _():
        rim_copy.wait_recv()
        padded[0:PAD, :] = rim[...].astype(F32)

    @pl.when(sp == 0)
    def _():
        padded[0:PAD, :] = jnp.zeros((PAD, C), F32)

    summed = jnp.zeros((L, C), F32)
    for j in range(taps_n):
        begin = PAD - (taps_n - 1) + j
        summed = summed + taps[j : j + 1, :] * padded[begin : begin + L, :]
    conv_all[tp, :, :] = (gate[...].astype(F32) * summed).astype(BF16)

    def mix_copy(which, buf, piece, r, send, target):
        block = buf.at[piece, mix_rows(r), :]
        return pltpu.make_async_remote_copy(
            src_ref=block,
            dst_ref=block,
            send_sem=send,
            recv_sem=mix_recv.at[which, piece, r],
            device_id={"tp": target},
        )

    def mix_own(which, buf, k, r):
        target = peer(k) if k else sib
        return mix_copy(which, buf, tp, r, mix_send.at[which, k, r], target)

    def mix_forward(which, buf, k, r):
        return mix_copy(which, buf, source(k), r, mix_relay.at[which, k, r], sib)

    def mix_wait(which, buf, piece, r):
        mix_copy(which, buf, piece, r, mix_send.at[which, 0, r], sib).wait_recv()

    for r in range(NM):
        for k in list(range(1, X)) + [0]:
            mix_own(0, conv_all, k, r).start()

    def step(dz, carry):
        def row_block(k, inner):
            def forward(r, c):
                relay(dz + 1, r)
                return c

            lax.fori_loop(k * NR // Y, (k + 1) * NR // Y, forward, 0)
            side = (y + k) % Y
            level = jnp.where(k == 0, z - dz, z - dz + 1)
            j = level * Y + side
            valid = jnp.where(k == 0, dz <= z, jnp.logical_or(level < z, side < y))

            @pl.when(valid)
            def _():
                @pl.when(k > 0)
                def _():
                    for r in range(NR):
                        if r < EX:
                            climbs = jnp.logical_and(level == 0, y == 1)

                            @pl.when(jnp.logical_not(jnp.logical_and(climbs, z == 0)))
                            def _():
                                kv_wait(j, r)

                            @pl.when(jnp.logical_and(climbs, jnp.logical_and(z > 0, has_up)))
                            def _():
                                extra(r).start()

                        else:
                            kv_wait(j, r)

                attend(j, False)

            return inner

        lax.fori_loop(0, Y, row_block, 0)
        return carry

    lax.fori_loop(1, z + 2, step, 0)

    def finish(i, carry):
        rows = mix_rows(i)
        for h in range(H):
            first_map = acc[h, 0, rows, :] / row_sum[h, 0, rows, :]
            second_map = acc[h, 1, rows, :] / row_sum[h, 1, rows, :]
            head_mix = first_map - lambdas[h] * second_map
            mean = jnp.mean(head_mix * head_mix, axis=1, keepdims=True)
            normed = head_mix * lax.rsqrt(mean + HEAD_EPS) * head_gain[...] * HEAD_SCALE
            attn_all[tp, rows, h * V : (h + 1) * V] = normed.astype(BF16)
        for k in list(range(1, X)) + [0]:
            mix_own(1, attn_all, k, i).start()
        return carry

    lax.fori_loop(0, NM, finish, 0)

    loads[6].wait()
    loads[7].wait()

    def gather(which, buf, r):
        for k in range(1, X):
            mix_wait(which, buf, source(k), r)
            mix_forward(which, buf, k, r).start()

    def gather_rest(which, buf, r):
        mix_wait(which, buf, sib, r)
        for k in range(1, X):
            mix_wait(which, buf, ((xi + k) % X) * 2 + (1 - core), r)

    def conv_part(r, carry):
        rows = mix_rows(r)
        gather(0, conv_all, r)
        gather_rest(0, conv_all, r)
        part = dot(conv_all[0, rows, :], wc[0:C, :])
        for t in range(1, T):
            part = part + dot(conv_all[t, rows, :], wc[t * C : (t + 1) * C, :])
        total[rows, :] = part
        return carry

    lax.fori_loop(0, NM, conv_part, 0)

    lanes = lax.broadcasted_iota(jnp.int32, (L, 128), 1)
    columns = jnp.zeros((L, 128), F32)
    for h in range(H):
        for c in range(2):
            value = row_max[h, c, :, :] + jnp.log(row_sum[h, c, :, :])
            columns = jnp.where(lanes == 2 * h + c, value, columns)
    turned_columns = jnp.transpose(columns)
    for h in range(H):
        lse[h] = turned_columns[2 * h : 2 * h + 2, :]

    def attn_part(r, carry):
        rows = mix_rows(r)
        gather(1, attn_all, r)
        gather_rest(1, attn_all, r)
        part = total[rows, :]
        for t in range(T):
            part = part + dot(attn_all[t, rows, :], wa[t * C : (t + 1) * C, :])
        out[rows, :] = part.astype(BF16)
        return carry

    lax.fori_loop(0, NM, attn_part, 0)

    for r in range(NR):
        for k in range(X):
            tok_own(k, r).wait_send()
        for k in range(1, X):
            tok_forward(k, r).wait_send()

    def drain(dz, carry):
        def inner(r, c):
            kv_send(dz, r, lambda copy: copy.wait_send())
            return c

        return lax.fori_loop(0, NR, inner, carry)

    lax.fori_loop(0, z + 1, drain, 0)
    if EX:

        @pl.when(jnp.logical_and(y == 1, has_up))
        def _():
            for r in range(EX):
                extra(r).wait_send()

    for which, buf in ((0, conv_all), (1, attn_all)):
        for r in range(NM):
            for k in range(X):
                mix_own(which, buf, k, r).wait_send()
            for k in range(1, X):
                mix_forward(which, buf, k, r).wait_send()

    @pl.when(sp + 1 < S)
    def _():
        rim_copy.wait_send()


def per_device(
    dims,
    tokens,
    norm_gain,
    query_weight,
    key_weight,
    value_weight,
    outer_gate_weight,
    inner_gate_weight,
    conv_input_weight,
    conv_taps,
    lambdas,
    head_gain,
    attn_out_weight,
    conv_out_weight,
):
    S, T, Z, Y = dims["S"], dims["T"], dims["Z"], dims["Y"]
    L, Dt = tokens.shape
    H = lambdas.shape[0]
    C = query_weight.shape[1]
    V = C // H
    hd = V // 2
    O = attn_out_weight.shape[1]
    Wd = norm_gain.shape[0]
    NR, NM, PAD = 4, 2, 16
    X = T // 2
    frequency = ROPE_BASE ** (-np.arange(hd // 2) * 2.0 / hd)
    freq = jnp.asarray(np.tile(frequency, 4)[None, :], F32)
    any_spec = pl.BlockSpec(memory_space=pl.ANY)
    vmem = pl.BlockSpec(memory_space=pltpu.VMEM)
    smem = pl.BlockSpec(memory_space=pltpu.SMEM)
    dma = pltpu.SemaphoreType.DMA
    mixed, lse = pl.pallas_call(
        functools.partial(kernel, dict(dims, H=H)),
        out_shape=(
            jax.ShapeDtypeStruct((L, O), BF16),
            jax.ShapeDtypeStruct((H, 2, L), F32),
        ),
        in_specs=[any_spec, vmem, vmem] + [any_spec] * 6 + [vmem, smem, vmem] + [any_spec] * 2,
        out_specs=(vmem, vmem),
        scratch_shapes=[
            pltpu.VMEM((T, L, Dt), BF16),
            pltpu.VMEM((L, Wd), BF16),
            pltpu.VMEM((L, 1), F32),
            pltpu.VMEM((L, V), F32),
            pltpu.VMEM((L, V), F32),
        ]
        + [pltpu.VMEM((Wd, C), BF16)] * 6
        + [pltpu.VMEM((T * C, O), BF16)] * 2
        + [
            pltpu.VMEM((S, L, 2 * C), BF16),
            pltpu.VMEM((H, 2, L, V), BF16),
            pltpu.VMEM((H, 2, L, 1), F32),
            pltpu.VMEM((H, 2, L, 1), F32),
            pltpu.VMEM((H, 2, L, V), F32),
            pltpu.VMEM((L, C), BF16),
            pltpu.VMEM((PAD + L, C), F32),
            pltpu.VMEM((PAD, C), BF16),
            pltpu.VMEM((PAD, C), BF16),
            pltpu.VMEM((T, L, C), BF16),
            pltpu.VMEM((T, L, C), BF16),
            pltpu.VMEM((L, O), F32),
            dma((8,)),
            dma,
            dma((T, NR)),
            dma((X, NR)),
            dma((X, NR)),
            dma((S, NR)),
            dma((Z, NR)),
            dma((Z, NR, max(Y - 1, 1))),
            dma((NR,)),
            dma((2,)),
            dma((2, T, NM)),
            dma((2, X, NM)),
            dma((2, X, NM)),
        ],
        compiler_params=pltpu.CompilerParams(
            collective_id=0, has_side_effects=True, vmem_limit_bytes=60 * 1024 * 1024
        ),
        name="mixer",
    )(
        tokens,
        norm_gain[None, :],
        freq,
        query_weight,
        key_weight,
        value_weight,
        outer_gate_weight,
        inner_gate_weight,
        conv_input_weight,
        conv_taps,
        lambdas,
        head_gain[None, :],
        attn_out_weight,
        conv_out_weight,
    )
    return mixed, lse


def solution(mesh):
    S, T = mesh.shape["sp"], mesh.shape["tp"]
    Y = max(d for d in range(1, S + 1) if S % d == 0 and d * d <= S)
    dims = {"S": S, "T": T, "Z": S // Y, "Y": Y}
    in_specs = (
        P("sp", "tp"),
        P(),
        P(None, "tp"),
        P(None, "tp"),
        P(None, "tp"),
        P(None, "tp"),
        P(None, "tp"),
        P(None, "tp"),
        P(None, "tp"),
        P("tp"),
        P(),
        P(None, "tp"),
        P(None, "tp"),
    )
    out_specs = (P("sp", "tp"), P("tp", None, "sp"))
    return jax.shard_map(
        functools.partial(per_device, dims),
        mesh=mesh,
        in_specs=in_specs,
        out_specs=out_specs,
        check_vma=False,
    )
```

profile of v0, /device:TPU:25, one launch (start us, length us, event | category | flops | bytes accessed | tf_op | source)
XLA Modules:
  0.0 78.1 jit_solution(17531902746700963711)
XLA Ops:
  0.6 75.0 %mixer.1 = (bf16[512,512]{1,0:T(8,128)(2,1)}, f32[2,2,512]{2,1,0:T(2,128)}) custom-call(bf16[512,512]{1,0:T(8,128)(2,1)} %tokens.1, f32[1,2048]{1,0:T(1,128)} %bitcast.2, f32[1,128]{1,0:T(1,128)} %constant.2.clone.freq, bf16[2048,256]{1,0:T(8,128)(2,1)} %wq_h.1, bf16[2048,256]{1,0:T(8,128)(2,1)} %wk_h.1, bf16[2048,256]{1,0:T(8,128)(2,1)} %wv_h.1, ...), custom_call_target="tpu_custom_call" | custom-call | tf_op jit(solution)/shard_map/mixer/pallas_call | solution.py:575
  75.7 0.0 copy-start
  75.7 1.9 %copy.18 = bf16[512,512]{1,0:T(8,128)(2,1)} copy(bf16[512,512]{1,0:T(8,128)(2,1)} %get-tuple-element.4) | data formatting | bytes 1048576
  77.5 0.0 copy-done
  77.5 0.6 copy.19
Async XLA Ops:
  75.7 1.9 %copy-start = (f32[2,2,512]{2,1,0:T(2,128)S(1)}, f32[2,2,512]{2,1,0:T(2,128)}, u32[]{:S(2)}) copy-start(f32[2,2,512]{2,1,0:T(2,128)} %get-tuple-element.5) | copy-start | bytes 24580
where the time goes:
time: 78.3 us; the launch traced here: 78.1 us
  Pallas kernels  75 us (96%)
  local copies, waits for them, and re-layouts  2.48 us (3%)
    pallas_call x1, Pallas kernels, per_device(): pl.pallas_call(functools.partial(kernel, dict(dims, H=H)), out_shape=(jax...  75 us
    unnamed x4, local copies, waits for them, and re-layouts  2.48 us

commit v1 on v0

--- a/solution.py
+++ b/solution.py
@@ -25,7 +25,7 @@
     return lax.dot_general(a, b, (((1,), (1,)), ((), ())), preferred_element_type=F32)
 
 
-def kernel(
+def ring_kernel(
     dims,
     tokens,
     gain,
@@ -540,7 +540,7 @@
         rim_copy.wait_send()
 
 
-def per_device(
+def ring_device(
     dims,
     tokens,
     norm_gain,
@@ -573,7 +573,7 @@
     smem = pl.BlockSpec(memory_space=pltpu.SMEM)
     dma = pltpu.SemaphoreType.DMA
     mixed, lse = pl.pallas_call(
-        functools.partial(kernel, dict(dims, H=H)),
+        functools.partial(ring_kernel, dict(dims, H=H)),
         out_shape=(
             jax.ShapeDtypeStruct((L, O), BF16),
             jax.ShapeDtypeStruct((H, 2, L), F32),
@@ -639,6 +639,747 @@
     return mixed, lse
 
 
+def pair_kernel(
+    dims,
+    tokens,
+    gain,
+    freq,
+    wq_h,
+    wk_h,
+    wv_h,
+    wo_h,
+    wi_h,
+    ws_h,
+    taps,
+    lambdas,
+    head_gain,
+    wa_h,
+    wc_h,
+    out,
+    lse,
+    tok,
+    scaled,
+    inv,
+    cos_t,
+    sin_t,
+    wq,
+    wk,
+    wv,
+    wo,
+    wi,
+    ws,
+    wa,
+    wc,
+    kvq,
+    row_max,
+    row_sum,
+    acc,
+    gate,
+    padded,
+    tail,
+    rim,
+    conv_all,
+    attn_all,
+    away,
+    lse_away,
+    lse_in,
+    total,
+    w_sem,
+    own_sem,
+    tok_recv,
+    tok_send,
+    tok_relay,
+    kv_recv,
+    swap_send,
+    cross_send,
+    side_send,
+    up_send,
+    rim_sem,
+    lse_sem,
+    mix_recv,
+    mix_send,
+    mix_relay,
+    at_recv,
+    at_send,
+    at_away,
+    at_relay,
+    at_relay_away,
+):
+    S, T, Z, Y, H = dims["S"], dims["T"], dims["Z"], dims["Y"], dims["H"]
+    L, Dt = tokens.shape
+    Wd = T * Dt
+    C = wq_h.shape[1]
+    V = C // H
+    hd = V // 2
+    NR = tok_recv.shape[1]
+    R = L // NR
+    NM = mix_recv.shape[1]
+    M = L // NM
+    G = M // R
+    X = T // 2
+    taps_n = taps.shape[0]
+    PAD = tail.shape[0]
+
+    sp = lax.axis_index("sp")
+    tp = lax.axis_index("tp")
+    z = sp // Y
+    y = sp % Y
+    pair = z // 2
+    a = z % 2
+    mate = sp + (1 - 2 * a) * Y
+    core = tp % 2
+    xi = tp // 2
+    sib = xi * 2 + (1 - core)
+    has_up = z + 2 - a < Z
+    has_down = pair > 0
+
+    def peer(k):
+        return ((xi + k) % X) * 2 + core
+
+    def source(k):
+        return ((xi - k + X) % X) * 2 + core
+
+    def source_sib(k):
+        return ((xi - k + X) % X) * 2 + (1 - core)
+
+    pairs = [(wk_h, wk), (wv_h, wv), (wq_h, wq), (wi_h, wi), (ws_h, ws), (wo_h, wo), (wc_h, wc), (wa_h, wa)]
+    own = pltpu.make_async_copy(tokens, tok.at[tp], own_sem)
+    own.start()
+    loads = [pltpu.make_async_copy(s, d, w_sem.at[i]) for i, (s, d) in enumerate(pairs)]
+    for load in loads:
+        load.start()
+
+    barrier = pltpu.get_barrier_semaphore()
+
+    def greet(target):
+        pl.semaphore_signal(barrier, inc=1, device_id=target)
+
+    for k in range(1, T):
+        greet({"tp": (tp + k) % T})
+    for k in range(X):
+        greet({"sp": mate, "tp": peer(k)})
+    for k in range(1, Y):
+        greet({"sp": z * Y + (y + k) % Y})
+    expect = (T - 1) + X + (Y - 1)
+    bridge_up = jnp.logical_and(a == 1, has_up)
+    bridge_down = jnp.logical_and(a == 0, has_down)
+    for near, step in (
+        (has_up, 2 * Y),
+        (has_down, -2 * Y),
+        (bridge_up, Y),
+        (bridge_down, -Y),
+        (sp + 1 < S, 1),
+        (sp > 0, -1),
+    ):
+        expect = expect + near.astype(jnp.int32)
+
+        @pl.when(near)
+        def _():
+            greet({"sp": sp + step})
+
+    pl.semaphore_wait(barrier, expect)
+
+    def tok_rows(r):
+        return pl.ds(pl.multiple_of(r * R, R), R)
+
+    def tok_copy(src, piece, r, send, target):
+        return pltpu.make_async_remote_copy(
+            src_ref=src,
+            dst_ref=tok.at[piece, tok_rows(r), :],
+            send_sem=send,
+            recv_sem=tok_recv.at[piece, r],
+            device_id={"tp": target},
+        )
+
+    def tok_own(k, r):
+        target = peer(k) if k else sib
+        return tok_copy(tokens.at[tok_rows(r), :], tp, r, tok_send.at[k, r], target)
+
+    def tok_forward(k, r):
+        piece = source(k)
+        return tok_copy(tok.at[piece, tok_rows(r), :], piece, r, tok_relay.at[k, r], sib)
+
+    def tok_wait(piece, r):
+        tok_copy(tok.at[piece, tok_rows(r), :], piece, r, tok_send.at[0, r], sib).wait_recv()
+
+    for r in range(NR):
+        for k in list(range(1, X)) + [0]:
+            tok_own(k, r).start()
+
+    lane = lax.broadcasted_iota(jnp.int32, (R, V), 1)
+    first = (lane % hd) < (hd // 2)
+
+    def table(r, carry):
+        base = sp * L + r * R
+        pos = (base + lax.broadcasted_iota(jnp.int32, (R, V), 0)).astype(F32)
+        angle = pos * freq[...]
+        sine = jnp.sin(angle)
+        cos_t[tok_rows(r), :] = jnp.cos(angle)
+        sin_t[tok_rows(r), :] = jnp.where(first, -sine, sine)
+        return carry
+
+    lax.fori_loop(0, NR, table, 0)
+
+    row_max[...] = jnp.full(row_max.shape, MASKED, F32)
+    row_sum[...] = jnp.zeros(row_sum.shape, F32)
+    acc[...] = jnp.zeros(acc.shape, F32)
+
+    def rotate(block, rows):
+        other = jnp.where(first, pltpu.roll(block, V - hd // 2, 1), pltpu.roll(block, hd // 2, 1))
+        return block * cos_t[rows, :] + other * sin_t[rows, :]
+
+    def kv_copy(src, j, r, send, target):
+        return pltpu.make_async_remote_copy(
+            src_ref=src,
+            dst_ref=kvq.at[j, r, pl.ds(0, 2)],
+            send_sem=send,
+            recv_sem=kv_recv.at[j, r],
+            device_id={"sp": target},
+        )
+
+    def swap(j, r):
+        return pltpu.make_async_remote_copy(
+            src_ref=kvq.at[S, r],
+            dst_ref=kvq.at[j, r],
+            send_sem=swap_send.at[r],
+            recv_sem=kv_recv.at[j, r],
+            device_id={"sp": mate},
+        )
+
+    def cross(r):
+        return kv_copy(kvq.at[S, r, pl.ds(0, 2)], sp, r, cross_send.at[r], sp + Y)
+
+    def level_block(level):
+        return level * Y + y
+
+    def up(level, r):
+        j = level_block(level)
+        return kv_copy(kvq.at[j, r, pl.ds(0, 2)], j, r, up_send.at[level, r], sp + 2 * Y)
+
+    def side(level, r, k):
+        j = level_block(level)
+        return kv_copy(
+            kvq.at[j, r, pl.ds(0, 2)], j, r, side_send.at[level, r, k - 1], z * Y + (y + k) % Y
+        )
+
+    def kv_wait(j, r):
+        kv_copy(kvq.at[j, r, pl.ds(0, 2)], j, r, cross_send.at[r], sp).wait_recv()
+
+    top = 2 * pair + 1
+
+    def spread(level, r, rises, act):
+        @pl.when(rises)
+        def _():
+            act(up(level, r))
+
+        for k in range(1, Y):
+
+            @pl.when(jnp.logical_or(level < top, y < (y + k) % Y))
+            def _():
+                act(side(level, r, k))
+
+    def start(copy):
+        copy.start()
+
+    def drain(copy):
+        copy.wait_send()
+
+    def send_own(r, act):
+        act(swap(sp, r))
+
+        @pl.when(bridge_up)
+        def _():
+            act(cross(r))
+
+        spread(z, r, has_up, act)
+
+    mate_level = z + 1 - 2 * a
+
+    def send_mate(r, act):
+        spread(mate_level, r, bridge_up, act)
+
+    def send_below(level, r, act):
+        spread(level, r, has_up, act)
+
+    def relay_mate(r):
+        swap(mate, r).wait_recv()
+        send_mate(r, start)
+
+    def relay_below(level, r):
+        kv_wait(level_block(level), r)
+        send_below(level, r, start)
+
+    own.wait()
+    for load in loads[:3]:
+        load.wait()
+    scale = hd ** (-0.5)
+
+    def chunk(r, carry):
+        rows = tok_rows(r)
+        for k in range(1, X):
+            tok_wait(source(k), r)
+            tok_forward(k, r).start()
+        tok_wait(sib, r)
+        for k in range(1, X):
+            tok_wait(source_sib(k), r)
+        squares = jnp.zeros((R, 1), F32)
+        for t in range(T):
+            block = tok[t, rows, :].astype(F32)
+            squares = squares + jnp.sum(block * block, axis=1, keepdims=True)
+            scaled[rows, t * Dt : (t + 1) * Dt] = (block * gain[:, t * Dt : (t + 1) * Dt]).astype(BF16)
+        inverse = lax.rsqrt(squares / Wd + NORM_EPS)
+        inv[rows, :] = inverse
+        left = scaled[rows, :]
+        keys = inverse * dot(left, wk[...])
+        values = inverse * dot(left, wv[...])
+        queries = inverse * dot(left, wq[...])
+        for h in range(H):
+            mine = a if h else 1 - a
+            slot = sp * mine + S * (1 - mine)
+            cols = slice(h * V, (h + 1) * V)
+            kvq[slot, r, 0] = rotate(keys[:, cols], rows).astype(BF16)
+            kvq[slot, r, 1] = jnp.transpose(values[:, cols]).astype(BF16)
+            turned = rotate(queries[:, cols], rows).astype(BF16).astype(F32) * scale
+            kvq[slot, r, 2] = jnp.transpose(turned).astype(BF16)
+        send_own(r, start)
+
+        @pl.when(r > 0)
+        def _():
+            relay_mate(r - 1)
+
+        return carry
+
+    lax.fori_loop(0, NR, chunk, 0)
+    relay_mate(NR - 1)
+
+    def relay_some(dp, begin, end):
+        @pl.when(dp <= pair)
+        def _():
+            for r in range(begin, end):
+                for b in range(2):
+                    relay_below(2 * (pair - dp) + b, r)
+
+    relay_some(1, 0, G // 2)
+
+    for load in loads[3:6]:
+        load.wait()
+
+    def mix_rows(r):
+        return pl.ds(pl.multiple_of(r * M, M), M)
+
+    def gate_chunk(r, carry):
+        rows = mix_rows(r)
+        inverse = inv[rows, :]
+        left = scaled[rows, :]
+        inner = (inverse * dot(left, wi[...])).astype(BF16)
+        signal = (inverse * dot(left, ws[...])).astype(BF16)
+        conv_in = (inner.astype(F32) * signal.astype(F32)).astype(BF16)
+        padded[pl.ds(pl.multiple_of(PAD + r * M, PAD), M), :] = conv_in.astype(F32)
+        gate[rows, :] = (inverse * dot(left, wo[...])).astype(BF16)
+        return carry
+
+    lax.fori_loop(0, NM, gate_chunk, 0)
+    tail[...] = padded[L : L + PAD, :].astype(BF16)
+    rim_copy = pltpu.make_async_remote_copy(
+        src_ref=tail,
+        dst_ref=rim,
+        send_sem=rim_sem.at[0],
+        recv_sem=rim_sem.at[1],
+        device_id={"sp": (sp + 1) % S},
+    )
+
+    @pl.when(sp + 1 < S)
+    def _():
+        rim_copy.start()
+
+    relay_some(1, G // 2, G)
+
+    key_row = lax.broadcasted_iota(jnp.int32, (M, M), 0)
+    query_lane = lax.broadcasted_iota(jnp.int32, (M, M), 1)
+    blank = jnp.zeros((hd, M), BF16)
+
+    def attend(j, half, tiles, diagonal=None):
+        keys = jnp.concatenate([kvq[j, G * half + g, 0] for g in range(G)], axis=0)
+        values = jnp.concatenate([kvq[j, G * half + g, 1] for g in range(G)], axis=1)
+        for b, part in tiles:
+            turned = jnp.concatenate(
+                [kvq[level_block(2 * pair + b), G * part + g, 2] for g in range(G)], axis=1
+            )
+            for c in range(2):
+                if c:
+                    right = jnp.concatenate([blank, turned[hd:]], axis=0)
+                else:
+                    right = jnp.concatenate([turned[:hd], blank], axis=0)
+                scores = dot(keys, right)
+                if (b, part) == diagonal:
+                    scores = jnp.where(key_row <= query_lane, scores, MASKED)
+                old_max = row_max[b, part, c]
+                new_max = jnp.maximum(old_max, jnp.max(scores, axis=0, keepdims=True))
+                weights = jnp.exp(scores - new_max)
+                fade = jnp.exp(old_max - new_max)
+                row_max[b, part, c] = new_max
+                row_sum[b, part, c] = fade * row_sum[b, part, c] + jnp.sum(weights, axis=0, keepdims=True)
+                acc[b, part, c] = fade * acc[b, part, c] + dot(values, weights.astype(BF16))
+
+    every = [(b, part) for b in range(2) for part in range(NM)]
+    for b in range(2):
+        for half in range(NM):
+            tiles = [(i, part) for i, part in every if (i, part) >= (b, half)]
+            attend(level_block(2 * pair + b), half, tiles, (b, half))
+
+    @pl.when(sp > 0)
+    def _():
+        rim_copy.wait_recv()
+        padded[0:PAD, :] = rim[...].astype(F32)
+
+    @pl.when(sp == 0)
+    def _():
+        padded[0:PAD, :] = jnp.zeros((PAD, C), F32)
+
+    summed = jnp.zeros((L, C), F32)
+    for j in range(taps_n):
+        begin = PAD - (taps_n - 1) + j
+        summed = summed + taps[j : j + 1, :] * padded[begin : begin + L, :]
+    conv_all[tp, :, :] = (gate[...].astype(F32) * summed).astype(BF16)
+
+    def mix_copy(piece, r, send, target):
+        block = conv_all.at[piece, mix_rows(r), :]
+        return pltpu.make_async_remote_copy(
+            src_ref=block,
+            dst_ref=block,
+            send_sem=send,
+            recv_sem=mix_recv.at[piece, r],
+            device_id={"tp": target},
+        )
+
+    def mix_own(k, r):
+        return mix_copy(tp, r, mix_send.at[k, r], peer(k) if k else sib)
+
+    def mix_forward(k, r):
+        return mix_copy(source(k), r, mix_relay.at[k, r], sib)
+
+    def mix_wait(piece, r):
+        mix_copy(piece, r, mix_send.at[0, r], sib).wait_recv()
+
+    for r in range(NM):
+        for k in list(range(1, X)) + [0]:
+            mix_own(k, r).start()
+
+    for k in range(1, Y):
+        other = (y + k) % Y
+        ahead = other < y
+        low = 2 * pair * Y + other
+        for r in range(NR):
+            kv_wait(low, r)
+
+        @pl.when(ahead)
+        def _():
+            for r in range(NR):
+                kv_wait(low + Y, r)
+
+        def beside(i, carry):
+            item = i // NM
+            half = i % NM
+            high = (item == 2).astype(jnp.int32)
+            late = 1 - (item == 1).astype(jnp.int32)
+            attend(low + high * Y, half, [(late, part) for part in range(NM)])
+            return carry
+
+        lax.fori_loop(0, NM * jnp.where(ahead, 3, 1), beside, 0)
+
+    def below(dp, carry):
+        def half_step(half, inner):
+            last = half == NM - 1
+            next_dp = dp + last.astype(jnp.int32)
+            next_r = G * ((half + 1) % NM)
+
+            def relay_next(g):
+                @pl.when(next_dp <= pair)
+                def _():
+                    for b in range(2):
+                        relay_below(2 * (pair - next_dp) + b, next_r + g)
+
+            def item(i, c):
+                k = i // 2
+                j = (2 * (pair - dp) + i % 2) * Y + (y + k) % Y
+
+                @pl.when(i == 2)
+                def _():
+                    for g in range(G // 2):
+                        relay_next(g)
+
+                @pl.when(k > 0)
+                def _():
+                    for g in range(G):
+                        kv_wait(j, G * half + g)
+
+                attend(j, half, every)
+                return c
+
+            lax.fori_loop(0, 2 * Y, item, 0)
+            for g in range(G // 2, G):
+                relay_next(g)
+            return inner
+
+        return lax.fori_loop(0, NM, half_step, carry)
+
+    lax.fori_loop(1, pair + 1, below, 0)
+
+    def at_copy(src, piece, h, r, send, target):
+        return pltpu.make_async_remote_copy(
+            src_ref=src,
+            dst_ref=attn_all.at[piece, h, mix_rows(r), :],
+            send_sem=send,
+            recv_sem=at_recv.at[piece, h, r],
+            device_id=target,
+        )
+
+    def at_own(k, r):
+        target = {"tp": peer(k) if k else sib}
+        return at_copy(attn_all.at[tp, a, mix_rows(r), :], tp, a, r, at_send.at[k, r], target)
+
+    def at_off(k, r):
+        target = {"sp": mate, "tp": peer(k)}
+        return at_copy(away.at[mix_rows(r), :], tp, a, r, at_away.at[k, r], target)
+
+    def at_forward(k, h, r, send):
+        piece = source(k)
+        return at_copy(attn_all.at[piece, h, mix_rows(r), :], piece, h, r, send, {"tp": sib})
+
+    def at_wait(piece, h, r):
+        at_copy(attn_all.at[piece, h, mix_rows(r), :], piece, h, r, at_send.at[0, r], {"tp": sib}).wait_recv()
+
+    def near_forward(k, r):
+        return at_forward(k, a, r, at_relay.at[k, r])
+
+    def far_forward(k, r):
+        return at_forward(k, 1 - a, r, at_relay_away.at[k, r])
+
+    def finished(b, part):
+        first_map = acc[b, part, 0] / row_sum[b, part, 0]
+        second_map = acc[b, part, 1] / row_sum[b, part, 1]
+        head_mix = first_map - lambdas[a] * second_map
+        mean = jnp.mean(head_mix * head_mix, axis=0, keepdims=True)
+        normed = head_mix * lax.rsqrt(mean + HEAD_EPS) * head_gain[...] * HEAD_SCALE
+        return jnp.transpose(normed).astype(BF16)
+
+    def log_total(b, part, c):
+        return row_max[b, part, c] + jnp.log(row_sum[b, part, c])
+
+    for part in range(NM):
+        away[part * M : (part + 1) * M, :] = finished(1 - a, part)
+        for k in list(range(1, X)) + [0]:
+            at_off(k, part).start()
+    for part in range(NM):
+        attn_all[tp, a, part * M : (part + 1) * M, :] = finished(a, part)
+        for k in list(range(1, X)) + [0]:
+            at_own(k, part).start()
+    for part in range(NM):
+        for c in range(2):
+            lse_away[c : c + 1, part * M : (part + 1) * M] = log_total(1 - a, part, c)
+            lse[a, c : c + 1, part * M : (part + 1) * M] = log_total(a, part, c)
+    lse_copy = pltpu.make_async_remote_copy(
+        src_ref=lse_away,
+        dst_ref=lse_in,
+        send_sem=lse_sem.at[0],
+        recv_sem=lse_sem.at[1],
+        device_id={"sp": mate},
+    )
+    lse_copy.start()
+
+    loads[6].wait()
+    loads[7].wait()
+
+    def conv_part(r, carry):
+        rows = mix_rows(r)
+        for k in range(1, X):
+            mix_wait(source(k), r)
+            mix_forward(k, r).start()
+        mix_wait(sib, r)
+        for k in range(1, X):
+            mix_wait(source_sib(k), r)
+        part = dot(conv_all[0, rows, :], wc[0:C, :])
+        for t in range(1, T):
+            part = part + dot(conv_all[t, rows, :], wc[t * C : (t + 1) * C, :])
+        total[rows, :] = part
+        return carry
+
+    lax.fori_loop(0, NM, conv_part, 0)
+
+    for r in range(NM):
+        for k in range(1, X):
+            at_wait(source(k), a, r)
+            near_forward(k, r).start()
+
+    def attn_part(r, carry):
+        rows = mix_rows(r)
+        for k in range(X):
+            at_wait(source(k), 1 - a, r)
+            far_forward(k, r).start()
+        for k in range(X):
+            at_wait(source_sib(k), a, r)
+        for k in range(X):
+            at_wait(source_sib(k), 1 - a, r)
+        part = total[rows, :]
+        for t in range(T):
+            both = jnp.concatenate([attn_all[t, h, rows, :] for h in range(H)], axis=1)
+            part = part + dot(both, wa[t * C : (t + 1) * C, :])
+        out[rows, :] = part.astype(BF16)
+        return carry
+
+    lax.fori_loop(0, NM, attn_part, 0)
+    lse_copy.wait_recv()
+    lse[1 - a] = lse_in[...]
+    lse_copy.wait_send()
+
+    for r in range(NR):
+        for k in range(X):
+            tok_own(k, r).wait_send()
+        for k in range(1, X):
+            tok_forward(k, r).wait_send()
+        send_own(r, drain)
+        send_mate(r, drain)
+
+    def drain_level(level, carry):
+        for r in range(NR):
+            send_below(level, r, drain)
+        return carry
+
+    lax.fori_loop(0, 2 * pair, drain_level, 0)
+
+    for r in range(NM):
+        for k in range(X):
+            mix_own(k, r).wait_send()
+            at_own(k, r).wait_send()
+            at_off(k, r).wait_send()
+            far_forward(k, r).wait_send()
+        for k in range(1, X):
+            mix_forward(k, r).wait_send()
+            near_forward(k, r).wait_send()
+
+    @pl.when(sp + 1 < S)
+    def _():
+        rim_copy.wait_send()
+
+
+def pair_device(
+    dims,
+    tokens,
+    norm_gain,
+    query_weight,
+    key_weight,
+    value_weight,
+    outer_gate_weight,
+    inner_gate_weight,
+    conv_input_weight,
+    conv_taps,
+    lambdas,
+    head_gain,
+    attn_out_weight,
+    conv_out_weight,
+):
+    S, T, Z, Y = dims["S"], dims["T"], dims["Z"], dims["Y"]
+    L, Dt = tokens.shape
+    H = lambdas.shape[0]
+    C = query_weight.shape[1]
+    V = C // H
+    hd = V // 2
+    O = attn_out_weight.shape[1]
+    Wd = norm_gain.shape[0]
+    R = V
+    M = 2 * R
+    NR, NM, PAD = L // R, L // M, 16
+    X = T // 2
+    frequency = ROPE_BASE ** (-np.arange(hd // 2) * 2.0 / hd)
+    freq = jnp.asarray(np.tile(frequency, 4)[None, :], F32)
+    any_spec = pl.BlockSpec(memory_space=pl.ANY)
+    vmem = pl.BlockSpec(memory_space=pltpu.VMEM)
+    smem = pl.BlockSpec(memory_space=pltpu.SMEM)
+    dma = pltpu.SemaphoreType.DMA
+    mixed, lse = pl.pallas_call(
+        functools.partial(pair_kernel, dict(dims, H=H)),
+        out_shape=(
+            jax.ShapeDtypeStruct((L, O), BF16),
+            jax.ShapeDtypeStruct((H, 2, L), F32),
+        ),
+        in_specs=[any_spec, vmem, vmem] + [any_spec] * 6 + [vmem, smem, vmem] + [any_spec] * 2,
+        out_specs=(vmem, vmem),
+        scratch_shapes=[
+            pltpu.VMEM((T, L, Dt), BF16),
+            pltpu.VMEM((L, Wd), BF16),
+            pltpu.VMEM((L, 1), F32),
+            pltpu.VMEM((L, V), F32),
+            pltpu.VMEM((L, V), F32),
+        ]
+        + [pltpu.VMEM((Wd, C), BF16)] * 6
+        + [pltpu.VMEM((T * C, O), BF16)] * 2
+        + [
+            pltpu.VMEM((S + 1, NR, 3, R, V), BF16),
+            pltpu.VMEM((2, NM, 2, 1, M), F32),
+            pltpu.VMEM((2, NM, 2, 1, M), F32),
+            pltpu.VMEM((2, NM, 2, V, M), F32),
+            pltpu.VMEM((L, C), BF16),
+            pltpu.VMEM((PAD + L, C), F32),
+            pltpu.VMEM((PAD, C), BF16),
+            pltpu.VMEM((PAD, C), BF16),
+            pltpu.VMEM((T, L, C), BF16),
+            pltpu.VMEM((T, H, L, V), BF16),
+            pltpu.VMEM((L, V), BF16),
+            pltpu.VMEM((2, L), F32),
+            pltpu.VMEM((2, L), F32),
+            pltpu.VMEM((L, O), F32),
+            dma((8,)),
+            dma,
+            dma((T, NR)),
+            dma((X, NR)),
+            dma((X, NR)),
+            dma((S, NR)),
+            dma((NR,)),
+            dma((NR,)),
+            dma((Z, NR, max(Y - 1, 1))),
+            dma((Z, NR)),
+            dma((2,)),
+            dma((2,)),
+            dma((T, NM)),
+            dma((X, NM)),
+            dma((X, NM)),
+            dma((T, H, NM)),
+            dma((X, NM)),
+            dma((X, NM)),
+            dma((X, NM)),
+            dma((X, NM)),
+        ],
+        compiler_params=pltpu.CompilerParams(
+            collective_id=0, has_side_effects=True, vmem_limit_bytes=60 * 1024 * 1024
+        ),
+        name="mixer",
+    )(
+        tokens,
+        norm_gain[None, :],
+        freq,
+        query_weight,
+        key_weight,
+        value_weight,
+        outer_gate_weight,
+        inner_gate_weight,
+        conv_input_weight,
+        conv_taps,
+        lambdas,
+        head_gain[:, None],
+        attn_out_weight,
+        conv_out_weight,
+    )
+    return mixed, lse
+
+
+def per_device(dims, *arrays):
+    tokens, query_weight, lambdas = arrays[0], arrays[2], arrays[9]
+    width = query_weight.shape[1] // lambdas.shape[0]
+    paired = lambdas.shape[0] == 2 and dims["Z"] % 2 == 0 and dims["T"] % 2 == 0
+    paired = paired and width == 128 and tokens.shape[0] % (2 * width) == 0
+    return (pair_device if paired else ring_device)(dims, *arrays)
+
+
 def solution(mesh):
     S, T = mesh.shape["sp"], mesh.shape["tp"]
     Y = max(d for d in range(1, S + 1) if S % d == 0 and d * d <= S)

time: 78.3 us -> 78.6 us (level)
  the two profiles are of different devices: /device:TPU:25 before, /device:TPU:21 now
where the time goes in v1:
time: 78.6 us; the launch traced here: 78.4 us
  Pallas kernels  73.9 us (94%)
  local copies, waits for them, and re-layouts  3.86 us (5%)
    pallas_call x1, Pallas kernels, pair_device(): pl.pallas_call(functools.partial(pair_kernel, dict(dims, H=H)), out_shape...  73.9 us
    unnamed x6, local copies, waits for them, and re-layouts  3.12 us

profile of v1, /device:TPU:21, one launch (start us, length us, event | category | flops | bytes accessed | tf_op | source)
XLA Modules:
  0.0 78.4 jit_solution(13779555284368405848)
XLA Ops:
  0.6 0.0 copy-start.1
  0.6 0.6 copy-done.1
  1.3 0.7 copy.16.head_gain
  2.0 73.9 %mixer.1 = (bf16[512,512]{1,0:T(8,128)(2,1)}, f32[2,2,512]{2,1,0:T(2,128)}) custom-call(bf16[512,512]{1,0:T(8,128)(2,1)} %tokens.1, f32[1,2048]{1,0:T(1,128)} %bitcast.2, f32[1,128]{1,0:T(1,128)} %constant.2.clone.freq, bf16[2048,256]{1,0:T(8,128)(2,1)} %wq_h.1, bf16[2048,256]{1,0:T(8,128)(2,1)} %wk_h.1, bf16[2048,256]{1,0:T(8,128)(2,1)} %wv_h.1, ...), custom_call_target="tpu_custom_call" | custom-call | tf_op jit(solution)/shard_map/mixer/pallas_call | solution.py:1299
  75.9 0.0 copy-start
  75.9 1.9 %copy.19 = bf16[512,512]{1,0:T(8,128)(2,1)} copy(bf16[512,512]{1,0:T(8,128)(2,1)} %get-tuple-element.4) | data formatting | bytes 1048576
  77.8 0.0 copy-done
  77.8 0.6 copy.20
Async XLA Ops:
  0.6 0.7 copy-start.1
  75.9 1.9 %copy-start = (f32[2,2,512]{2,1,0:T(2,128)S(1)}, f32[2,2,512]{2,1,0:T(2,128)}, u32[]{:S(2)}) copy-start(f32[2,2,512]{2,1,0:T(2,128)} %get-tuple-element.5) | copy-start | bytes 24580
